TPU v7x, 256 devices: a whole 4x4x8 slice. The times are simulated.
256 devices in a mesh: ep: 32 (over z, x), tp: 8 (over y, core).
Axes of the slice: x: 4, y: 4, z: 8, core: 2. Of those that a mesh axis runs over, the one named last changes fastest.
Arguments:
- hidden: bfloat16 [1024, 4096], P('ep', 'tp'), may hold values from -6 to 6
- norm_gain: float32 [4096], P('tp'), may hold values from 0.1 to 1.9
- expert_ids: int32 [1024, 8], P('ep'), may hold values from 0 to 63, as said below
- route_weights: float32 [1024, 8], P('ep'), may hold values from 0.1 to 1
- lengths: int32 [128], P('ep'), may hold values from 1 to 8, as said below
- gate_proj: bfloat16 [64, 4096, 1024], P('ep', None, 'tp'), may hold values from -0.09375 to 0.09375
- up_proj: bfloat16 [64, 4096, 1024], P('ep', None, 'tp'), may hold values from -0.09375 to 0.09375
- down_proj: bfloat16 [64, 1024, 4096], P('ep', 'tp'), may hold values from -0.1875 to 0.1875
- shared_gate: bfloat16 [4096, 1024], P(None, 'tp'), may hold values from -0.09375 to 0.09375
- shared_up: bfloat16 [4096, 1024], P(None, 'tp'), may hold values from -0.09375 to 0.09375
- shared_down: bfloat16 [1024, 4096], P('tp'), may hold values from -0.1875 to 0.1875
Outputs:
- mixed: bfloat16 [1024, 4096], P('ep', 'tp')
Inputs may be any that keep to these rules, and one draw needn't show every extreme that they name: `expert_ids`: among the 32 rows of one index of ep (an aligned block), no expert is named more than 12 times, and in every block one expert is named exactly 12 times; each row names 8 different experts. `lengths`: each sequence has 1 to 8 live slots; on some index of ep all 4 sequences have 8 live slots.
All inputs are finite; a program needn't handle non-finite values.
Results may differ from a plain program's by a relative error of at most 0.015.
Values may be sent and summed in bfloat16 or wider, within the bound.
A program may use at most 128 MiB of HBM per device.

v0:
```python
import jax
import jax.numpy as jnp
from jax import lax
from jax.sharding import PartitionSpec as P

epsilon = 1e-06


def in_order(tiles, dim):
    lengths = list(tiles.shape[1:])
    lengths[dim] *= tiles.shape[0]
    return jnp.moveaxis(tiles, 0, dim).reshape(lengths)


def sent_to_all(value, axis):
    size = lax.axis_size(axis)
    return lax.all_to_all(
        jnp.broadcast_to(value[None], (size, *value.shape)), axis, 0, 0, tiled=True
    )


def gathered_copies(value, axis, dim):
    return in_order(sent_to_all(value, axis), dim)


def over_copies(value, axis):
    everything = sent_to_all(value, axis)
    return jnp.sum(everything, axis=0)


def cut_along(value, dim, size):
    before, after = (value.shape[:dim], value.shape[dim + 1 :])
    return jnp.moveaxis(value.reshape(*before, size, -1, *after), dim, 0)


def summed_on_arrival(value, axis, dim):
    tiles = cut_along(value, dim, lax.axis_size(axis))
    arrived = lax.all_to_all(tiles, axis, split_axis=0, concat_axis=0, tiled=True)
    return arrived.astype(jnp.float32).sum(axis=0)


def expert_inner(arrived, gate_proj, up_proj):
    gate_value = jnp.einsum(
        "gecd,edf->gecf", arrived, gate_proj, preferred_element_type=jnp.float32
    )
    up_value = jnp.einsum("gecd,edf->gecf", arrived, up_proj, preferred_element_type=jnp.float32)
    return (jax.nn.silu(gate_value) * up_value).astype(jnp.bfloat16)


def widen_rows(arrived):
    flat_rows = arrived.reshape(-1, arrived.shape[-1])
    widened = gathered_copies(flat_rows, "tp", 1)
    return widened.reshape(arrived.shape[:-1] + (widened.shape[1],))


def dispatch_plan(source_rows, expert_ids, is_live, expert_count, capacity, local_experts):
    slot_count, top_count = expert_ids.shape
    flat_ids = expert_ids.reshape(-1)
    flat_live = jnp.repeat(is_live, top_count)
    hit_matrix = (
        (flat_ids[:, None] == jnp.arange(expert_count, dtype=jnp.int32)[None, :])
        & flat_live[:, None]
    ).astype(jnp.int32)
    earlier = jnp.cumsum(hit_matrix, axis=0) - hit_matrix
    position = jnp.sum(hit_matrix * earlier, axis=1)
    total_slots = expert_count * capacity
    slot_index = jnp.where(flat_live, flat_ids * capacity + position, total_slots)
    chooser = jnp.any(
        slot_index.reshape(slot_count, top_count)[None, :, :]
        == jnp.arange(total_slots, dtype=jnp.int32)[:, None, None],
        axis=2,
    )
    outgoing = jnp.dot(
        chooser.astype(jnp.bfloat16), source_rows, preferred_element_type=jnp.float32
    ).astype(jnp.bfloat16)
    outgoing = outgoing.reshape(lax.axis_size("ep"), local_experts, capacity, source_rows.shape[1])
    return (outgoing, slot_index)


def collect_rows(returned, slot_index, mixing):
    slot_count, top_count = mixing.shape
    back_flat = returned.reshape(-1, returned.shape[3])
    total_slots = back_flat.shape[0]
    picked = jnp.take(back_flat, jnp.minimum(slot_index, total_slots - 1), axis=0)
    picked = picked.reshape(slot_count, top_count, back_flat.shape[1])
    return jnp.sum(mixing[:, :, None] * picked, axis=1)


def body(
    hidden,
    norm_gain,
    expert_ids,
    route_weights,
    lengths,
    gate_proj,
    up_proj,
    down_proj,
    shared_gate,
    shared_up,
    shared_down,
):
    slot_count = hidden.shape[0]
    top_count = expert_ids.shape[1]
    span_size = slot_count // lengths.shape[0]
    local_experts = gate_proj.shape[0]
    expert_count = local_experts * lax.axis_size("ep")
    capacity = min(
        slot_count, max(2, (3 * slot_count * top_count + expert_count - 1) // expert_count)
    )
    model_width = hidden.shape[1] * lax.axis_size("tp")
    values = hidden.astype(jnp.float32)
    squares = over_copies(jnp.sum(values * values, axis=1), "tp")
    row_scale = lax.rsqrt(squares / model_width + epsilon)
    normed = (values * row_scale[:, None] * norm_gain[None, :]).astype(jnp.bfloat16)
    full_rows = gathered_copies(normed, "tp", 1)
    offsets = jnp.arange(slot_count, dtype=jnp.int32) % span_size
    is_live = offsets < jnp.repeat(lengths, span_size)
    mixing = jnp.where(is_live[:, None], route_weights, 0.0)
    shared_inner = (
        jax.nn.silu(jnp.dot(full_rows, shared_gate, preferred_element_type=jnp.float32))
        * jnp.dot(full_rows, shared_up, preferred_element_type=jnp.float32)
    ).astype(jnp.bfloat16)
    shared_part = jnp.dot(shared_inner, shared_down, preferred_element_type=jnp.float32)
    outgoing, slot_index = dispatch_plan(
        normed, expert_ids, is_live, expert_count, capacity, local_experts
    )
    down_share = lax.all_to_all(down_proj, "tp", split_axis=2, concat_axis=1, tiled=True)
    inner_value = expert_inner(
        widen_rows(lax.all_to_all(outgoing, "ep", split_axis=0, concat_axis=0, tiled=True)),
        gate_proj,
        up_proj,
    )
    inner_whole = gathered_copies(inner_value, "tp", 3)
    result = jnp.einsum(
        "gecf,efd->gecd", inner_whole, down_share, preferred_element_type=jnp.float32
    )
    returned = lax.all_to_all(
        result.astype(jnp.bfloat16), "ep", split_axis=0, concat_axis=0, tiled=True
    ).astype(result.dtype)
    routed = collect_rows(returned, slot_index, mixing)
    combined = routed + summed_on_arrival(shared_part.astype(jnp.bfloat16), "tp", 1)
    return jnp.where(is_live[:, None], combined, 0.0).astype(jnp.bfloat16)


def solution(mesh):
    placed = (
        P("ep", "tp"),
        P("tp"),
        P("ep", None),
        P("ep", None),
        P("ep"),
        P("ep", None, "tp"),
        P("ep", None, "tp"),
        P("ep", "tp", None),
        P(None, "tp"),
        P(None, "tp"),
        P("tp", None),
    )
    return jax.shard_map(body, mesh=mesh, in_specs=placed, out_specs=P("ep", "tp"), check_vma=False)
```

profile of v0, /device:TPU:2, one launch (start us, length us, event | category | flops | bytes accessed | tf_op | source)
XLA Modules:
  0.0 256.2 jit_solution(8316562800688118385)
XLA Ops:
  0.0 1.0 fusion.39
  1.6 4.5 %all-to-all-start = ((f32[8,1,32]{2,1,0:T(1,128)}), f32[8,1,32]{2,1,0:T(1,128)S(1)}, u32[]{:S(2)}, u32[]{:S(2)}) async-start(f32[8,1,32]{2,1,0:T(1,128)} %broadcast_in_dim.97), calls=%async_computation | async-start | bytes 8192 | tf_op jit(solution)/shard_map/all_to_all | solution.py:17
  12.2 1.3 convolution_convert_fusion.1
  13.5 1.2 reshape.159
  15.6 33.9 %all_to_all.54 = bf16[32,2,12,512]{3,1,2,0:T(2,128)(2,1)} all-to-all(bf16[32,2,12,512]{3,1,2,0:T(2,128)(2,1)S(1)} %copy.99), channel_id=1, replica_groups=mesh['ep'=32,'tp'=8] {'ep'}, dimensions={0} | all-to-all | bytes 1572864 | tf_op jit(solution)/shard_map/all_to_all | solution.py:129
  50.2 4.4 %all-to-all-start.6 = ((bf16[8,32,512]{2,1,0:T(8,128)(2,1)}), bf16[8,32,512]{2,1,0:T(8,128)(2,1)S(1)}, u32[]{:S(2)}, u32[]{:S(2)}) async-start(bf16[8,32,512]{2,1,0:T(8,128)(2,1)} %broadcast_in_dim.103), calls=%async_computation.6 | async-start | bytes 524288 | tf_op jit(solution)/shard_map/all_to_all | solution.py:17
  54.6 1.3 copy.100
  56.0 1.1 broadcast_in_dim.98
  57.0 5.1 %all-to-all-done.6 = bf16[8,32,512]{2,1,0:T(8,128)(2,1)S(1)} async-done(((bf16[8,32,512]{2,1,0:T(8,128)(2,1)}), bf16[8,32,512]{2,1,0:T(8,128)(2,1)S(1)}, u32[]{:S(2)}, u32[]{:S(2)}) %all-to-all-start.6) | async-done | bytes 262176 | tf_op jit(solution)/shard_map/all_to_all | solution.py:17
  62.1 4.4 %broadcast_in_dim.99 = bf16[8,768,512]{2,1,0:T(8,128)(2,1)} broadcast(bf16[768,512]{1,0:T(8,128)(2,1)} %broadcast_in_dim.98), dimensions={1,2} | broadcast | bytes 7077888 | tf_op jit(solution)/shard_map/broadcast_in_dim | solution.py:18
  66.6 4.7 %all-to-all-start.2 = ((bf16[8,768,512]{2,1,0:T(8,128)(2,1)}), bf16[8,768,512]{2,1,0:T(8,128)(2,1)}, u32[]{:S(2)}, u32[]{:S(2)}) async-start(bf16[8,768,512]{2,1,0:T(8,128)(2,1)} %broadcast_in_dim.99), calls=%async_computation.2 | async-start | bytes 12582912 | tf_op jit(solution)/shard_map/all_to_all | solution.py:17
  71.3 6.2 %copy.105 = bf16[2,128,4096]{1,0,2:T(2,128)(2,1)} copy(bf16[2,128,4096]{2,1,0:T(8,128)(2,1)} %param.18) | data formatting | bytes 4194304 | tf_op args[7]
  77.5 66.0 %all-to-all-done.2 = bf16[8,768,512]{2,1,0:T(8,128)(2,1)} async-done(((bf16[8,768,512]{2,1,0:T(8,128)(2,1)}), bf16[8,768,512]{2,1,0:T(8,128)(2,1)}, u32[]{:S(2)}, u32[]{:S(2)}) %all-to-all-start.2) | async-done | bytes 6291488 | tf_op jit(solution)/shard_map/all_to_all | solution.py:17
  143.4 4.4 %all-to-all-start.4 = ((bf16[2,128,4096]{1,0,2:T(2,128)(2,1)}), bf16[2,128,4096]{1,0,2:T(2,128)(2,1)}, u32[]{:S(2)}, u32[]{:S(2)}) async-start(bf16[2,128,4096]{1,0,2:T(2,128)(2,1)} %copy.105), calls=%async_computation.4 | async-start | bytes 4194304 | tf_op jit(solution)/shard_map/all_to_all | solution.py:127
  147.8 9.0 %copy.101 = bf16[768,8,512]{2,1,0:T(8,128)(2,1)} copy(bf16[768,8,512]{2,0,1:T(8,128)(2,1)} %bitcast.2) | data formatting | bytes 12582912 | tf_op jit(solution)/shard_map/transpose | solution.py:12
  156.8 12.0 %reshape_reshape.3 = bf16[32,2,12,4096]{3,2,1,0:T(8,128)(2,1)} reshape(bf16[768,8,512]{2,1,0:T(8,128)(2,1)} %copy.101) | data formatting | bytes 12582912 | tf_op jit(solution)/shard_map/reshape;reshape | solution.py:53
  168.9 7.9 %fusion.15 = f32[32,2,12,128]{3,0,2,1:T(8,128)S(1)} fusion(bf16[2,4096,128]{2,1,0:T(8,128)(2,1)S(1)} %copy-done, bf16[32,2,12,4096]{3,2,1,0:T(8,128)(2,1)} %reshape_reshape.3), kind=kOutput, calls=%fused_computation.14 | convolution fusion | flops 805306368 | bytes 8781824 | tf_op jit(solution)/shard_map/gecd,edf->gecf/dot_general | solution.py:43
  176.8 4.3 %fusion.30 = bf16[32,2,12,128]{3,0,2,1:T(8,128)(2,1)S(1)} fusion(bf16[2,4096,128]{2,1,0:T(8,128)(2,1)S(1)} %copy-done.5, bf16[32,2,12,4096]{3,2,1,0:T(8,128)(2,1)S(1)} %copy-done.1, f32[32,2,12,128]{3,0,2,1:T(8,128)S(1)} %fusion.15), kind=kOutput, calls=%fused_computation.17 | convolution fusion | flops 805896192 | bytes 8978432 | tf_op jit(solution)/shard_map/gecd,edf->gecf/dot_general | solution.py:46
  181.1 1.5 broadcast_in_dim.100
  182.6 4.8 %all-to-all-start.3 = ((bf16[8,32,2,12,128]{4,1,3,2,0:T(8,128)(2,1)}), bf16[8,32,2,12,128]{4,1,3,2,0:T(8,128)(2,1)}, u32[]{:S(2)}, u32[]{:S(2)}) async-start(bf16[8,32,2,12,128]{4,1,3,2,0:T(8,128)(2,1)} %broadcast_in_dim.100), calls=%async_computation.3 | async-start | bytes 3145728 | tf_op jit(solution)/shard_map/all_to_all | solution.py:17
  188.7 2.1 convolution_convert_fusion
  191.5 6.1 %copy.106 = bf16[2,128,8,512]{3,1,2,0:T(8,128)(2,1)} copy(bf16[2,128,8,512]{1,0,3,2:T(2,128)(2,1)} %bitcast.10) | data formatting | bytes 4194304 | tf_op jit(solution)/shard_map/all_to_all | solution.py:127
  197.6 11.4 %all-to-all-done.3 = bf16[8,32,2,12,128]{4,1,3,2,0:T(8,128)(2,1)} async-done(((bf16[8,32,2,12,128]{4,1,3,2,0:T(8,128)(2,1)}), bf16[8,32,2,12,128]{4,1,3,2,0:T(8,128)(2,1)}, u32[]{:S(2)}, u32[]{:S(2)}) %all-to-all-start.3) | async-done | bytes 1572896 | tf_op jit(solution)/shard_map/all_to_all | solution.py:17
  209.1 3.4 %all-to-all-start.7 = ((bf16[8,32,512]{2,1,0:T(8,128)(2,1)}), bf16[8,32,512]{2,1,0:T(8,128)(2,1)S(1)}, u32[]{:S(2)}, u32[]{:S(2)}) async-start(bf16[8,32,512]{2,1,0:T(8,128)(2,1)} %bitcast.94), calls=%async_computation.7 | async-start | bytes 524288 | tf_op jit(solution)/shard_map/all_to_all | solution.py:38
  212.5 3.0 %fusion.12 = bf16[32,2,12,512]{3,0,2,1:T(8,128)(2,1)S(1)} fusion(bf16[2,1024,512,1]{2,1,3,0:T(8,128)(2,1)} %bitcast.97, bf16[8,32,2,12,128]{4,1,3,2,0:T(8,128)(2,1)} %all-to-all-done.3), kind=kOutput, calls=%fused_computation.13 | convolution fusion | flops 805699584 | bytes 4456448 | tf_op jit(solution)/shard_map/gecf,efd->gecd/dot_general | solution.py:134
  215.6 1.7 copy.107
  217.2 2.7 %all-to-all-done.7 = bf16[8,32,512]{2,1,0:T(8,128)(2,1)S(1)} async-done(((bf16[8,32,512]{2,1,0:T(8,128)(2,1)}), bf16[8,32,512]{2,1,0:T(8,128)(2,1)S(1)}, u32[]{:S(2)}, u32[]{:S(2)}) %all-to-all-start.7) | async-done | bytes 262176 | tf_op jit(solution)/shard_map/all_to_all | solution.py:38
  219.9 5.6 %all-to-all-start.5 = ((bf16[32,2,12,512]{3,1,2,0:T(2,128)(2,1)}), bf16[32,2,12,512]{3,1,2,0:T(2,128)(2,1)S(1)}, u32[]{:S(2)}, u32[]{:S(2)}) async-start(bf16[32,2,12,512]{3,1,2,0:T(2,128)(2,1)} %copy.107), calls=%async_computation.5 | async-start | bytes 1572864 | tf_op jit(solution)/shard_map/all_to_all | solution.py:137
  225.9 21.7 %all-to-all-done.5 = bf16[32,2,12,512]{3,1,2,0:T(2,128)(2,1)S(1)} async-done(((bf16[32,2,12,512]{3,1,2,0:T(2,128)(2,1)}), bf16[32,2,12,512]{3,1,2,0:T(2,128)(2,1)S(1)}, u32[]{:S(2)}, u32[]{:S(2)}) %all-to-all-start.5) | async-done | bytes 786464 | tf_op jit(solution)/shard_map/all_to_all | solution.py:137
  247.8 2.3 copy.109
  250.1 2.6 reshape.167
  252.7 2.6 %gather_fusion = f32[256,512]{1,0:T(8,128)S(1)} fusion(f32[768,512]{1,0:T(8,128)} %reshape.167, s32[1024]{0:T(1024)S(1)} %pad_clamp_fusion), kind=kCustom, calls=%fused_computation | custom fusion | bytes 1049600 | tf_op jit(solution)/shard_map/jit(_take)/gather | solution.py:84
  (57 shorter events, 11.8 us)
Async XLA Ops:
  0.0 168.9 %copy-start = (bf16[2,4096,128]{2,1,0:T(8,128)(2,1)S(1)}, bf16[2,4096,128]{2,1,0:T(8,128)(2,1)}, u32[]{:S(2)}) copy-start(bf16[2,4096,128]{2,1,0:T(8,128)(2,1)} %param.16) | copy-start | bytes 6291460
  1.6 9.7 %all-to-all-start = ((f32[8,1,32]{2,1,0:T(1,128)}), f32[8,1,32]{2,1,0:T(1,128)S(1)}, u32[]{:S(2)}, u32[]{:S(2)}) async-start(f32[8,1,32]{2,1,0:T(1,128)} %broadcast_in_dim.97), calls=%async_computation | async-start | bytes 8192 | tf_op jit(solution)/shard_map/all_to_all | solution.py:17
  50.2 11.9 %all-to-all-start.6 = ((bf16[8,32,512]{2,1,0:T(8,128)(2,1)}), bf16[8,32,512]{2,1,0:T(8,128)(2,1)S(1)}, u32[]{:S(2)}, u32[]{:S(2)}) async-start(bf16[8,32,512]{2,1,0:T(8,128)(2,1)} %broadcast_in_dim.103), calls=%async_computation.6 | async-start | bytes 524288 | tf_op jit(solution)/shard_map/all_to_all | solution.py:17
  62.1 4.4 %copy-start.3 = (bf16[8,32,512]{2,1,0:T(8,128)(2,1)}, bf16[8,32,512]{2,1,0:T(8,128)(2,1)S(1)}, u32[]{:S(2)}) copy-start(bf16[8,32,512]{2,1,0:T(8,128)(2,1)S(1)} %all-to-all-done.6) | copy-start | bytes 786436
  66.6 76.9 %all-to-all-start.2 = ((bf16[8,768,512]{2,1,0:T(8,128)(2,1)}), bf16[8,768,512]{2,1,0:T(8,128)(2,1)}, u32[]{:S(2)}, u32[]{:S(2)}) async-start(bf16[8,768,512]{2,1,0:T(8,128)(2,1)} %broadcast_in_dim.99), calls=%async_computation.2 | async-start | bytes 12582912 | tf_op jit(solution)/shard_map/all_to_all | solution.py:17
  143.4 37.7 %all-to-all-start.4 = ((bf16[2,128,4096]{1,0,2:T(2,128)(2,1)}), bf16[2,128,4096]{1,0,2:T(2,128)(2,1)}, u32[]{:S(2)}, u32[]{:S(2)}) async-start(bf16[2,128,4096]{1,0,2:T(2,128)(2,1)} %copy.105), calls=%async_computation.4 | async-start | bytes 4194304 | tf_op jit(solution)/shard_map/all_to_all | solution.py:127
  168.9 7.9 %copy-start.1 = (bf16[32,2,12,4096]{3,2,1,0:T(8,128)(2,1)S(1)}, bf16[32,2,12,4096]{3,2,1,0:T(8,128)(2,1)}, u32[]{:S(2)}) copy-start(bf16[32,2,12,4096]{3,2,1,0:T(8,128)(2,1)} %reshape_reshape.3) | copy-start | bytes 18874372
  168.9 7.9 %copy-start.5 = (bf16[2,4096,128]{2,1,0:T(8,128)(2,1)S(1)}, bf16[2,4096,128]{2,1,0:T(8,128)(2,1)}, u32[]{:S(2)}) copy-start(bf16[2,4096,128]{2,1,0:T(8,128)(2,1)} %param.17) | copy-start | bytes 6291460
  182.6 5.8 %copy-start.2 = (bf16[4096,128]{1,0:T(8,128)(2,1)S(1)}, bf16[4096,128]{1,0:T(8,128)(2,1)}, u32[]{:S(2)}) copy-start(bf16[4096,128]{1,0:T(8,128)(2,1)} %param.19) | copy-start | bytes 3145732
  182.6 26.5 %all-to-all-start.3 = ((bf16[8,32,2,12,128]{4,1,3,2,0:T(8,128)(2,1)}), bf16[8,32,2,12,128]{4,1,3,2,0:T(8,128)(2,1)}, u32[]{:S(2)}, u32[]{:S(2)}) async-start(bf16[8,32,2,12,128]{4,1,3,2,0:T(8,128)(2,1)} %broadcast_in_dim.100), calls=%async_computation.3 | async-start | bytes 3145728 | tf_op jit(solution)/shard_map/all_to_all | solution.py:17
  209.1 10.8 %all-to-all-start.7 = ((bf16[8,32,512]{2,1,0:T(8,128)(2,1)}), bf16[8,32,512]{2,1,0:T(8,128)(2,1)S(1)}, u32[]{:S(2)}, u32[]{:S(2)}) async-start(bf16[8,32,512]{2,1,0:T(8,128)(2,1)} %bitcast.94), calls=%async_computation.7 | async-start | bytes 524288 | tf_op jit(solution)/shard_map/all_to_all | solution.py:38
  215.5 10.2 %copy-start.4 = (f32[32,8]{0,1:T(8,128)S(1)}, f32[32,8]{0,1:T(8,128)}, u32[]{:S(2)}) copy-start(f32[32,8]{0,1:T(8,128)} %param.14) | copy-start | bytes 3076
  219.9 27.7 %all-to-all-start.5 = ((bf16[32,2,12,512]{3,1,2,0:T(2,128)(2,1)}), bf16[32,2,12,512]{3,1,2,0:T(2,128)(2,1)S(1)}, u32[]{:S(2)}, u32[]{:S(2)}) async-start(bf16[32,2,12,512]{3,1,2,0:T(2,128)(2,1)} %copy.107), calls=%async_computation.5 | async-start | bytes 1572864 | tf_op jit(solution)/shard_map/all_to_all | solution.py:137
where the time goes:
time: 258 us; the launch traced here: 256 us
  waiting for transfers between devices  108 us (42%)
  local copies, waits for them, and re-layouts  59.4 us (23%)
  blocking collectives  33.9 us (13%)
  starting transfers between devices  31.8 us (12%)
  matrix products  18.9 us (7%)
  other arithmetic  4.39 us (2%)
    all_to_all x4, waiting for transfers between devices, sent_to_all(): lax.all_to_all(jnp.broadcast_to(value[None], (size, *value.shape)), axis,...  83.2 us
    all_to_all x1, blocking collectives, body(): lax.all_to_all(outgoing, 'ep', split_axis=0, concat_axis=0, tiled=True)  33.9 us
    all_to_all x1, waiting for transfers between devices, body(): lax.all_to_all(result.astype(jnp.bfloat16), 'ep', split_axis=0, concat_ax...  21.7 us
    all_to_all x4, starting transfers between devices, sent_to_all(): lax.all_to_all(jnp.broadcast_to(value[None], (size, *value.shape)), axis,...  18.4 us
    another operation x1, local copies, waits for them, and re-layouts, widen_rows(): return widened.reshape(arrived.shape[:-1] + (widened.shape[1],))  12 us
    transpose x1, local copies, waits for them, and re-layouts, in_order(): return jnp.moveaxis(tiles, 0, dim).reshape(lengths)  9.03 us
    broadcast_in_dim x5, local copies, waits for them, and re-layouts, sent_to_all(): jnp.broadcast_to(value[None], (size, *value.shape))  8.3 us
    dot_general x1, matrix products, expert_inner(): jnp.einsum('gecd,edf->gecf', arrived, gate_proj, preferred_element_type=j...  7.85 us
  transfers between devices with their start and end apart: 7, of which 6 were waited for; matrix products, arithmetic and copies ran while one was open for 24% of the time, Pallas kernels for 0%

commit v1 on v0

--- a/solution.py
+++ b/solution.py
@@ -4,6 +4,13 @@
 from jax.sharding import PartitionSpec as P
 
 epsilon = 1e-06
+
+
+def stacked_exchange(shard, name, split, join):
+    n_dev = lax.axis_size(name)
+    blocks = jnp.stack(jnp.split(shard, n_dev, axis=split), axis=0)
+    blocks = lax.all_to_all(blocks, name, split_axis=0, concat_axis=0)
+    return jnp.concatenate(blocks, axis=join)
 
 
 def in_order(tiles, dim):
@@ -124,7 +131,7 @@
     outgoing, slot_index = dispatch_plan(
         normed, expert_ids, is_live, expert_count, capacity, local_experts
     )
-    down_share = lax.all_to_all(down_proj, "tp", split_axis=2, concat_axis=1, tiled=True)
+    down_share = stacked_exchange(down_proj, "tp", 2, 1)
     inner_value = expert_inner(
         widen_rows(lax.all_to_all(outgoing, "ep", split_axis=0, concat_axis=0, tiled=True)),
         gate_proj,

time: 258 us -> 258 us (level)
  waiting for transfers between devices: 108 us -> 103 us
  local copies, waits for them, and re-layouts: 59.4 us -> 63.7 us
    all_to_all x1 -> x0, local copies, waits for them, and re-layouts: 6.14 us -> none  [body(): lax.all_to_all(down_proj, 'tp', split_axis=2, concat_axis=1, tiled=True)]
    unnamed x15 -> x21, local copies, waits for them, and re-layouts: 7.02 us -> 12.6 us
    all_to_all x4, waiting for transfers between devices: 83.2 us -> 79 us  [sent_to_all(): lax.all_to_all(jnp.broadcast_to(value[None], (size, *value.shape)), axis,...]
    reshape x0 -> x1, local copies, waits for them, and re-layouts: none -> 3.13 us  [stacked_exchange(): return jnp.concatenate(blocks, axis=join)]
  transfers between devices with their start and end apart: 7 -> 7, of which waited for: 6 -> 6; matrix products, arithmetic and copies ran while one was open for 24% -> 26% of each run, Pallas kernels for 0% -> 0%
where the time goes in v1:
time: 258 us; the launch traced here: 256 us
  waiting for transfers between devices  103 us (40%)
  local copies, waits for them, and re-layouts  63.7 us (25%)
  blocking collectives  33.9 us (13%)
  starting transfers between devices  31.8 us (12%)
  matrix products  18.8 us (7%)
  other arithmetic  4.39 us (2%)
    all_to_all x4, waiting for transfers between devices, sent_to_all(): lax.all_to_all(jnp.broadcast_to(value[None], (size, *value.shape)), axis,...  79 us
    all_to_all x1, blocking collectives, body(): lax.all_to_all(outgoing, 'ep', split_axis=0, concat_axis=0, tiled=True)  33.9 us
    all_to_all x1, waiting for transfers between devices, body(): lax.all_to_all(result.astype(jnp.bfloat16), 'ep', split_axis=0, concat_ax...  21.7 us
    all_to_all x4, starting transfers between devices, sent_to_all(): lax.all_to_all(jnp.broadcast_to(value[None], (size, *value.shape)), axis,...  18.4 us
    unnamed x21, local copies, waits for them, and re-layouts  12.6 us
    another operation x1, local copies, waits for them, and re-layouts, widen_rows(): return widened.reshape(arrived.shape[:-1] + (widened.shape[1],))  12 us
    transpose x1, local copies, waits for them, and re-layouts, in_order(): return jnp.moveaxis(tiles, 0, dim).reshape(lengths)  9.03 us
    broadcast_in_dim x5, local copies, waits for them, and re-layouts, sent_to_all(): jnp.broadcast_to(value[None], (size, *value.shape))  8.3 us
  transfers between devices with their start and end apart: 7, of which 6 were waited for; matrix products, arithmetic and copies ran while one was open for 26% of the time, Pallas kernels for 0%

profile of v1, /device:TPU:2, one launch (start us, length us, event | category | flops | bytes accessed | tf_op | source)
XLA Modules:
  0.0 256.2 jit_solution(266614098668414876)
XLA Ops:
  1.6 4.5 %all-to-all-start.1 = ((f32[8,1,32]{2,1,0:T(1,128)}), f32[8,1,32]{2,1,0:T(1,128)S(1)}, u32[]{:S(2)}, u32[]{:S(2)}) async-start(f32[8,1,32]{2,1,0:T(1,128)} %broadcast_in_dim.97), calls=%async_computation.1 | async-start | bytes 8192 | tf_op jit(solution)/shard_map/all_to_all | solution.py:24
  15.6 33.9 %all_to_all.41 = bf16[32,2,12,512]{3,1,2,0:T(2,128)(2,1)} all-to-all(bf16[32,2,12,512]{3,1,2,0:T(2,128)(2,1)S(1)} %copy.96), channel_id=1, replica_groups=mesh['ep'=32,'tp'=8] {'ep'}, dimensions={0} | all-to-all | bytes 1572864 | tf_op jit(solution)/shard_map/all_to_all | solution.py:136
  50.2 4.4 %all-to-all-start.6 = ((bf16[8,32,512]{2,1,0:T(8,128)(2,1)}), bf16[8,32,512]{2,1,0:T(8,128)(2,1)S(1)}, u32[]{:S(2)}, u32[]{:S(2)}) async-start(bf16[8,32,512]{2,1,0:T(8,128)(2,1)} %broadcast_in_dim.103), calls=%async_computation.6 | async-start | bytes 524288 | tf_op jit(solution)/shard_map/all_to_all | solution.py:24
  57.0 5.1 %all-to-all-done.6 = bf16[8,32,512]{2,1,0:T(8,128)(2,1)S(1)} async-done(((bf16[8,32,512]{2,1,0:T(8,128)(2,1)}), bf16[8,32,512]{2,1,0:T(8,128)(2,1)S(1)}, u32[]{:S(2)}, u32[]{:S(2)}) %all-to-all-start.6) | async-done | bytes 262176 | tf_op jit(solution)/shard_map/all_to_all | solution.py:24
  62.1 4.4 %broadcast_in_dim.99 = bf16[8,768,512]{2,1,0:T(8,128)(2,1)} broadcast(bf16[768,512]{1,0:T(8,128)(2,1)} %broadcast_in_dim.98), dimensions={1,2} | broadcast | bytes 7077888 | tf_op jit(solution)/shard_map/broadcast_in_dim | solution.py:25
  66.6 4.7 %all-to-all-start.3 = ((bf16[8,768,512]{2,1,0:T(8,128)(2,1)}), bf16[8,768,512]{2,1,0:T(8,128)(2,1)}, u32[]{:S(2)}, u32[]{:S(2)}) async-start(bf16[8,768,512]{2,1,0:T(8,128)(2,1)} %broadcast_in_dim.99), calls=%async_computation.3 | async-start | bytes 12582912 | tf_op jit(solution)/shard_map/all_to_all | solution.py:24
  73.0 1.7 bitcast_dynamic-update-slice_fusion.6
  74.6 1.7 bitcast_dynamic-update-slice_fusion.5
  76.3 1.7 bitcast_dynamic-update-slice_fusion.4
  78.0 1.7 bitcast_dynamic-update-slice_fusion.3
  79.7 1.7 bitcast_dynamic-update-slice_fusion.2
  81.4 1.7 bitcast_dynamic-update-slice_fusion.1
  83.1 1.7 bitcast_dynamic-update-slice_fusion
  84.7 58.7 %all-to-all-done.3 = bf16[8,768,512]{2,1,0:T(8,128)(2,1)} async-done(((bf16[8,768,512]{2,1,0:T(8,128)(2,1)}), bf16[8,768,512]{2,1,0:T(8,128)(2,1)}, u32[]{:S(2)}, u32[]{:S(2)}) %all-to-all-start.3) | async-done | bytes 6291488 | tf_op jit(solution)/shard_map/all_to_all | solution.py:24
  143.4 4.4 %all-to-all-start = ((bf16[8,2,128,512]{3,2,1,0:T(8,128)(2,1)}), bf16[8,2,128,512]{3,2,1,0:T(8,128)(2,1)}, u32[]{:S(2)}, u32[]{:S(2)}) async-start(bf16[8,2,128,512]{3,2,1,0:T(8,128)(2,1)} %bitcast_dynamic-update-slice_fusion), calls=%async_computation | async-start | bytes 4194304 | tf_op jit(solution)/shard_map/all_to_all | solution.py:12
  147.8 9.0 %copy.98 = bf16[768,8,512]{2,1,0:T(8,128)(2,1)} copy(bf16[768,8,512]{2,0,1:T(8,128)(2,1)} %bitcast.14) | data formatting | bytes 12582912 | tf_op jit(solution)/shard_map/transpose | solution.py:19
  156.8 12.0 %reshape_reshape.3 = bf16[32,2,12,4096]{3,2,1,0:T(8,128)(2,1)} reshape(bf16[768,8,512]{2,1,0:T(8,128)(2,1)} %copy.98) | data formatting | bytes 12582912 | tf_op jit(solution)/shard_map/reshape;reshape | solution.py:60
  168.9 7.9 %fusion.15 = f32[32,2,12,128]{3,0,2,1:T(8,128)S(1)} fusion(bf16[2,4096,128]{2,1,0:T(8,128)(2,1)S(1)} %copy-done, bf16[32,2,12,4096]{3,2,1,0:T(8,128)(2,1)} %reshape_reshape.3), kind=kOutput, calls=%fused_computation.14 | convolution fusion | flops 805306368 | bytes 8781824 | tf_op jit(solution)/shard_map/gecd,edf->gecf/dot_general | solution.py:50
  176.8 4.3 %fusion.30 = bf16[32,2,12,128]{3,0,2,1:T(8,128)(2,1)S(1)} fusion(bf16[2,4096,128]{2,1,0:T(8,128)(2,1)S(1)} %copy-done.5, bf16[32,2,12,4096]{3,2,1,0:T(8,128)(2,1)S(1)} %copy-done.1, f32[32,2,12,128]{3,0,2,1:T(8,128)S(1)} %fusion.15), kind=kOutput, calls=%fused_computation.17 | convolution fusion | flops 805896192 | bytes 8978432 | tf_op jit(solution)/shard_map/gecd,edf->gecf/dot_general | solution.py:53
  182.6 4.8 %all-to-all-start.4 = ((bf16[8,32,2,12,128]{4,1,3,2,0:T(8,128)(2,1)}), bf16[8,32,2,12,128]{4,1,3,2,0:T(8,128)(2,1)}, u32[]{:S(2)}, u32[]{:S(2)}) async-start(bf16[8,32,2,12,128]{4,1,3,2,0:T(8,128)(2,1)} %broadcast_in_dim.100), calls=%async_computation.4 | async-start | bytes 3145728 | tf_op jit(solution)/shard_map/all_to_all | solution.py:24
  188.7 2.1 convolution_convert_fusion
  191.5 3.1 %copy.94 = bf16[2,8,128,512]{3,2,1,0:T(8,128)(2,1)} copy(bf16[2,8,128,512]{3,2,0,1:T(8,128)(2,1)} %bitcast.9) | data formatting | bytes 4194304 | tf_op jit(solution)/shard_map/reshape | solution.py:13
  194.6 14.4 %all-to-all-done.4 = bf16[8,32,2,12,128]{4,1,3,2,0:T(8,128)(2,1)} async-done(((bf16[8,32,2,12,128]{4,1,3,2,0:T(8,128)(2,1)}), bf16[8,32,2,12,128]{4,1,3,2,0:T(8,128)(2,1)}, u32[]{:S(2)}, u32[]{:S(2)}) %all-to-all-start.4) | async-done | bytes 1572896 | tf_op jit(solution)/shard_map/all_to_all | solution.py:24
  209.1 3.4 %all-to-all-start.7 = ((bf16[8,32,512]{2,1,0:T(8,128)(2,1)}), bf16[8,32,512]{2,1,0:T(8,128)(2,1)S(1)}, u32[]{:S(2)}, u32[]{:S(2)}) async-start(bf16[8,32,512]{2,1,0:T(8,128)(2,1)} %bitcast.108), calls=%async_computation.7 | async-start | bytes 524288 | tf_op jit(solution)/shard_map/all_to_all | solution.py:45
  212.5 3.0 %fusion.12 = bf16[32,2,12,512]{3,0,2,1:T(8,128)(2,1)S(1)} fusion(bf16[2,1024,512,1]{2,1,3,0:T(8,128)(2,1)} %bitcast.111, bf16[8,32,2,12,128]{4,1,3,2,0:T(8,128)(2,1)} %all-to-all-done.4), kind=kOutput, calls=%fused_computation.13 | convolution fusion | flops 805699584 | bytes 4456448 | tf_op jit(solution)/shard_map/gecf,efd->gecd/dot_general | solution.py:141
  215.5 1.7 copy.102
  217.2 2.7 %all-to-all-done.7 = bf16[8,32,512]{2,1,0:T(8,128)(2,1)S(1)} async-done(((bf16[8,32,512]{2,1,0:T(8,128)(2,1)}), bf16[8,32,512]{2,1,0:T(8,128)(2,1)S(1)}, u32[]{:S(2)}, u32[]{:S(2)}) %all-to-all-start.7) | async-done | bytes 262176 | tf_op jit(solution)/shard_map/all_to_all | solution.py:45
  219.9 5.6 %all-to-all-start.5 = ((bf16[32,2,12,512]{3,1,2,0:T(2,128)(2,1)}), bf16[32,2,12,512]{3,1,2,0:T(2,128)(2,1)S(1)}, u32[]{:S(2)}, u32[]{:S(2)}) async-start(bf16[32,2,12,512]{3,1,2,0:T(2,128)(2,1)} %copy.102), calls=%async_computation.5 | async-start | bytes 1572864 | tf_op jit(solution)/shard_map/all_to_all | solution.py:144
  225.9 21.7 %all-to-all-done.5 = bf16[32,2,12,512]{3,1,2,0:T(2,128)(2,1)S(1)} async-done(((bf16[32,2,12,512]{3,1,2,0:T(2,128)(2,1)}), bf16[32,2,12,512]{3,1,2,0:T(2,128)(2,1)S(1)}, u32[]{:S(2)}, u32[]{:S(2)}) %all-to-all-start.5) | async-done | bytes 786464 | tf_op jit(solution)/shard_map/all_to_all | solution.py:144
  247.9 2.3 copy.104
  250.1 2.6 reshape.175
  252.7 2.6 %gather_fusion = f32[256,512]{1,0:T(8,128)S(1)} fusion(f32[768,512]{1,0:T(8,128)} %reshape.175, s32[1024]{0:T(1024)S(1)} %pad_clamp_fusion), kind=kCustom, calls=%fused_computation | custom fusion | bytes 1049600 | tf_op jit(solution)/shard_map/jit(_take)/gather | solution.py:91
  (64 shorter events, 20.9 us)
Async XLA Ops:
  0.0 168.9 %copy-start = (bf16[2,4096,128]{2,1,0:T(8,128)(2,1)S(1)}, bf16[2,4096,128]{2,1,0:T(8,128)(2,1)}, u32[]{:S(2)}) copy-start(bf16[2,4096,128]{2,1,0:T(8,128)(2,1)} %param.16) | copy-start | bytes 6291460
  1.6 9.7 %all-to-all-start.1 = ((f32[8,1,32]{2,1,0:T(1,128)}), f32[8,1,32]{2,1,0:T(1,128)S(1)}, u32[]{:S(2)}, u32[]{:S(2)}) async-start(f32[8,1,32]{2,1,0:T(1,128)} %broadcast_in_dim.97), calls=%async_computation.1 | async-start | bytes 8192 | tf_op jit(solution)/shard_map/all_to_all | solution.py:24
  50.2 11.9 %all-to-all-start.6 = ((bf16[8,32,512]{2,1,0:T(8,128)(2,1)}), bf16[8,32,512]{2,1,0:T(8,128)(2,1)S(1)}, u32[]{:S(2)}, u32[]{:S(2)}) async-start(bf16[8,32,512]{2,1,0:T(8,128)(2,1)} %broadcast_in_dim.103), calls=%async_computation.6 | async-start | bytes 524288 | tf_op jit(solution)/shard_map/all_to_all | solution.py:24
  62.1 4.4 %copy-start.3 = (bf16[8,32,512]{2,1,0:T(8,128)(2,1)}, bf16[8,32,512]{2,1,0:T(8,128)(2,1)S(1)}, u32[]{:S(2)}) copy-start(bf16[8,32,512]{2,1,0:T(8,128)(2,1)S(1)} %all-to-all-done.6) | copy-start | bytes 786436
  66.6 76.9 %all-to-all-start.3 = ((bf16[8,768,512]{2,1,0:T(8,128)(2,1)}), bf16[8,768,512]{2,1,0:T(8,128)(2,1)}, u32[]{:S(2)}, u32[]{:S(2)}) async-start(bf16[8,768,512]{2,1,0:T(8,128)(2,1)} %broadcast_in_dim.99), calls=%async_computation.3 | async-start | bytes 12582912 | tf_op jit(solution)/shard_map/all_to_all | solution.py:24
  143.4 37.7 %all-to-all-start = ((bf16[8,2,128,512]{3,2,1,0:T(8,128)(2,1)}), bf16[8,2,128,512]{3,2,1,0:T(8,128)(2,1)}, u32[]{:S(2)}, u32[]{:S(2)}) async-start(bf16[8,2,128,512]{3,2,1,0:T(8,128)(2,1)} %bitcast_dynamic-update-slice_fusion), calls=%async_computation | async-start | bytes 4194304 | tf_op jit(solution)/shard_map/all_to_all | solution.py:12
  168.9 7.9 %copy-start.1 = (bf16[32,2,12,4096]{3,2,1,0:T(8,128)(2,1)S(1)}, bf16[32,2,12,4096]{3,2,1,0:T(8,128)(2,1)}, u32[]{:S(2)}) copy-start(bf16[32,2,12,4096]{3,2,1,0:T(8,128)(2,1)} %reshape_reshape.3) | copy-start | bytes 18874372
  168.9 7.9 %copy-start.5 = (bf16[2,4096,128]{2,1,0:T(8,128)(2,1)S(1)}, bf16[2,4096,128]{2,1,0:T(8,128)(2,1)}, u32[]{:S(2)}) copy-start(bf16[2,4096,128]{2,1,0:T(8,128)(2,1)} %param.17) | copy-start | bytes 6291460
  182.6 5.8 %copy-start.2 = (bf16[4096,128]{1,0:T(8,128)(2,1)S(1)}, bf16[4096,128]{1,0:T(8,128)(2,1)}, u32[]{:S(2)}) copy-start(bf16[4096,128]{1,0:T(8,128)(2,1)} %param.19) | copy-start | bytes 3145732
  182.6 26.5 %all-to-all-start.4 = ((bf16[8,32,2,12,128]{4,1,3,2,0:T(8,128)(2,1)}), bf16[8,32,2,12,128]{4,1,3,2,0:T(8,128)(2,1)}, u32[]{:S(2)}, u32[]{:S(2)}) async-start(bf16[8,32,2,12,128]{4,1,3,2,0:T(8,128)(2,1)} %broadcast_in_dim.100), calls=%async_computation.4 | async-start | bytes 3145728 | tf_op jit(solution)/shard_map/all_to_all | solution.py:24
  209.1 10.8 %all-to-all-start.7 = ((bf16[8,32,512]{2,1,0:T(8,128)(2,1)}), bf16[8,32,512]{2,1,0:T(8,128)(2,1)S(1)}, u32[]{:S(2)}, u32[]{:S(2)}) async-start(bf16[8,32,512]{2,1,0:T(8,128)(2,1)} %bitcast.108), calls=%async_computation.7 | async-start | bytes 524288 | tf_op jit(solution)/shard_map/all_to_all | solution.py:45
  215.5 10.2 %copy-start.4 = (f32[32,8]{0,1:T(8,128)S(1)}, f32[32,8]{0,1:T(8,128)}, u32[]{:S(2)}) copy-start(f32[32,8]{0,1:T(8,128)} %param.14) | copy-start | bytes 3076
  219.9 27.7 %all-to-all-start.5 = ((bf16[32,2,12,512]{3,1,2,0:T(2,128)(2,1)}), bf16[32,2,12,512]{3,1,2,0:T(2,128)(2,1)S(1)}, u32[]{:S(2)}, u32[]{:S(2)}) async-start(bf16[32,2,12,512]{3,1,2,0:T(2,128)(2,1)} %copy.102), calls=%async_computation.5 | async-start | bytes 1572864 | tf_op jit(solution)/shard_map/all_to_all | solution.py:144
